TPU v7x, 128 devices: a whole 4x4x4 slice. The times are simulated.
128 devices in a mesh: sp: 64 (over z, y, x), tp: 2 (over core).
Axes of the slice: x: 4, y: 4, z: 4, core: 2. Of those that a mesh axis runs over, the one named last changes fastest.
Arguments:
- query_small: bfloat16 [24576, 2, 128], P('sp', 'tp'), may hold values from -8 to 8
- key_small: bfloat16 [24576, 2, 128], P('sp', 'tp'), may hold values from -8 to 8
- value_small: bfloat16 [24576, 2, 128], P('sp', 'tp'), may hold values from -6 to 6
- query_large: bfloat16 [24576, 2, 256], P('sp', 'tp'), may hold values from -8 to 8
- key_large: bfloat16 [24576, 2, 256], P('sp', 'tp'), may hold values from -8 to 8
- value_large: bfloat16 [24576, 2, 128], P('sp', 'tp'), may hold values from -6 to 6
- lambdas: float32 [2, 2], P('tp'), may hold values from 0.3 to 0.8
- slopes: float32 [2, 2], P('tp'), as said below
- head_gain: bfloat16 [128], replicated, may hold values from 0.099609375 to 1.8984375
- residual: bfloat16 [24576, 2048], P(('sp', 'tp')), may hold values from -6 to 6
- out_weight: bfloat16 [512, 2048], replicated, may hold values from -0.25 to 0.25
- norm_gains: bfloat16 [2, 2048], replicated, may hold values from 0.099609375 to 1.8984375
- routes: int32 [24576, 2], P(('sp', 'tp')), may hold values from 0 to 63, as said below
- route_weights: float32 [24576, 2], P(('sp', 'tp')), may hold values from 0.1 to 1
- gate_weight: bfloat16 [64, 2048, 1024], P('sp', None, 'tp'), may hold values from -0.125 to 0.125
- up_weight: bfloat16 [64, 2048, 1024], P('sp', None, 'tp'), may hold values from -0.125 to 0.125
- down_weight: bfloat16 [64, 1024, 2048], P('sp', 'tp'), may hold values from -0.1875 to 0.1875
Outputs:
- layer_out: bfloat16 [24576, 2048], P(('sp', 'tp'))
Inputs may be any that keep to these rules, and one draw needn't show every extreme that they name: `slopes`: positive. `routes`: each token names two different experts of one group of 16 consecutive expert numbers. In each aligned block of 192 rows (the tokens of one device) no expert is named more than 12 times, and some expert is named exactly 12 times in every block.
All inputs are finite; a program needn't handle non-finite values.
Results may differ from a plain program's by a relative error of at most 0.011.
Values may be sent and summed in bfloat16 or wider, within the bound.
No kernel may reach another device: no remote copies, remote signals or barrier semaphores. Data moves between devices by JAX's collectives and lax.ppermute only.
A program may use at most 128 MiB of HBM per device.

v0:
```python
import math

import jax
import jax.numpy as jnp
from jax import lax
from jax.sharding import PartitionSpec as P

residual_gain = 8.0**0.25
epsilon = 1e-05
masked_score = -1e30


def cut_along(shard, dim, size):
    before, after = (shard.shape[:dim], shard.shape[dim + 1 :])
    return jnp.moveaxis(shard.reshape(*before, size, -1, *after), dim, 0)


def sent_and_summed(shard, axis, dim):
    blocks = cut_along(shard, dim, lax.axis_size(axis))
    arrived = lax.all_to_all(blocks, axis, split_axis=0, concat_axis=0, tiled=True)
    return arrived.astype(jnp.float32).sum(axis=0)


def layer_norm(values, gain_row):
    average = jnp.mean(values, axis=-1, keepdims=True)
    centred = values - average
    variance = jnp.mean(centred * centred, axis=-1, keepdims=True)
    return centred * lax.rsqrt(variance + epsilon) * gain_row.astype(jnp.float32)


def empty_state(head_count, length, value_size):
    return (
        jnp.full((head_count, 2, length), masked_score, jnp.float32),
        jnp.zeros((head_count, 2, length), jnp.float32),
        jnp.zeros((head_count, 2, length, value_size), jnp.float32),
    )


def advance(carried, keyset, valueset, queries, slope_row, positions):
    head_count = queries.shape[1]
    key_width = queries.shape[3]
    length = keyset.shape[0]
    block_rows = math.gcd(length, 512)
    blocks = length // block_rows
    key_blocks = keyset.reshape(blocks, block_rows, head_count, 2, key_width)
    value_blocks = valueset.reshape(blocks, block_rows, head_count, -1)
    score_scale = key_width ** (-0.5)
    last_query = positions[-1]

    def update(running, inputs):
        key_block, value_block, number = inputs
        first_key = number * block_rows

        def compute(current):
            running_max, running_sum, running_acc = current
            scores = (
                jnp.einsum(
                    "qhmd,khmd->hmqk", queries, key_block, preferred_element_type=jnp.float32
                )
                * score_scale
            )
            distance = (positions[:, None] - (first_key + jnp.arange(block_rows))[None, :]).astype(
                jnp.float32
            )
            scores = scores - slope_row[:, None, None, None] * distance
            scores = jnp.where(distance >= 0, scores, masked_score)
            new_max = jnp.maximum(running_max, jnp.max(scores, axis=-1))
            factor = jnp.exp(running_max - new_max)
            weights = jnp.exp(scores - new_max[..., None])
            new_sum = running_sum * factor + jnp.sum(weights, axis=-1)
            product = jnp.einsum(
                "hmqk,khe->hmqe",
                weights.astype(jnp.bfloat16),
                value_block,
                preferred_element_type=jnp.float32,
            )
            return (new_max, new_sum, running_acc * factor[..., None] + product)

        return (lax.cond(first_key <= last_query, compute, lambda current: current, running), None)

    carried, _ = lax.scan(update, carried, (key_blocks, value_blocks, jnp.arange(blocks)))
    return carried


def finish(carried, lambda_row, head_gain):
    running_max, running_sum, running_acc = carried
    mixture = running_acc / running_sum[..., None]
    head_out = mixture[:, 0] - lambda_row[:, None, None] * mixture[:, 1]
    scaled = head_out * lax.rsqrt(jnp.mean(head_out * head_out, axis=-1, keepdims=True) + epsilon)
    scaled = scaled * head_gain.astype(jnp.float32)
    return jnp.transpose(scaled, (1, 0, 2))


def shards(
    query_small,
    key_small,
    value_small,
    query_large,
    key_large,
    value_large,
    lambdas,
    slopes,
    head_gain,
    residual,
    out_weight,
    norm_gains,
    routes,
    route_weights,
    gate_weight,
    up_weight,
    down_weight,
):
    length = query_small.shape[0]
    head_count = query_small.shape[1]
    value_size = value_small.shape[2]
    positions = lax.axis_index("sp") * length + jnp.arange(length)
    small_queries = query_small.reshape(length, head_count, 2, -1)
    large_queries = query_large.reshape(length, head_count, 2, -1)
    small_start = empty_state(head_count, length, value_size)
    large_start = empty_state(head_count, length, value_size)

    def fold_large(carried, pieces):
        return advance(carried, pieces[0], pieces[1], large_queries, slopes[:, 1], positions)

    pieces = (
        lax.all_gather(key_small, "sp", axis=0, tiled=True),
        lax.all_gather(value_small, "sp", axis=0, tiled=True),
        lax.all_gather(key_large, "sp", axis=0, tiled=True),
        lax.all_gather(value_large, "sp", axis=0, tiled=True),
    )
    small_state = advance(small_start, pieces[0], pieces[1], small_queries, slopes[:, 0], positions)
    large_state = fold_large(large_start, (pieces[2], pieces[3]))
    attended = jnp.stack(
        [
            finish(small_state, lambdas[:, 0], head_gain),
            finish(large_state, lambdas[:, 1], head_gain),
        ],
        axis=2,
    ).astype(jnp.bfloat16)
    core_count = lax.axis_size("tp")
    row_count = length // core_count
    regrouped = lax.all_to_all(attended, "tp", split_axis=0, concat_axis=1, tiled=True)
    projected = jnp.dot(
        regrouped.reshape(row_count, -1), out_weight, preferred_element_type=jnp.float32
    )
    middle = layer_norm(
        residual_gain * residual.astype(jnp.float32) + projected, norm_gains[0]
    ).astype(jnp.bfloat16)
    experts = lax.axis_size("sp")
    capacity = 4 * row_count // experts
    features = middle.shape[1]
    chosen = routes.reshape(-1)
    matches = (chosen[:, None] == jnp.arange(experts)[None, :]).astype(jnp.int32)
    earlier = jnp.cumsum(matches, axis=0) - matches
    target = chosen * capacity + jnp.sum(earlier * matches, axis=1)
    selector = jnp.any(
        target.reshape(row_count, 2)[None, :, :] == jnp.arange(experts * capacity)[:, None, None],
        axis=2,
    ).astype(jnp.bfloat16)
    outgoing = jnp.dot(selector, middle, preferred_element_type=jnp.float32).astype(jnp.bfloat16)
    outgoing = outgoing.reshape(experts, capacity, features)
    arrived = lax.all_to_all(outgoing, "sp", split_axis=0, concat_axis=0, tiled=True)
    paired = lax.all_gather(arrived, "tp", axis=0, tiled=True).reshape(-1, features)
    gate_in = jnp.dot(paired, gate_weight[0], preferred_element_type=jnp.float32)
    upward = jnp.dot(paired, up_weight[0], preferred_element_type=jnp.float32)
    hidden = (jax.nn.silu(gate_in) * upward).astype(jnp.bfloat16)
    partial_value = jnp.dot(hidden, down_weight[0], preferred_element_type=jnp.float32).astype(
        jnp.bfloat16
    )
    summed = sent_and_summed(
        lax.optimization_barrier(partial_value).astype(jnp.float32).astype(jnp.bfloat16), "tp", 0
    ).astype(jnp.bfloat16)
    returned = lax.all_to_all(
        summed.reshape(experts, capacity, features), "sp", split_axis=0, concat_axis=0, tiled=True
    )
    expert_out = returned.reshape(experts * capacity, features)
    picked = jnp.take(expert_out, target, axis=0).reshape(row_count, 2, features)
    moe_sum = jnp.sum(route_weights[:, :, None] * picked.astype(jnp.float32), axis=1)
    return layer_norm(residual_gain * middle.astype(jnp.float32) + moe_sum, norm_gains[1]).astype(
        jnp.bfloat16
    )


def solution(mesh):
    placed = (
        P("sp", "tp", None),
        P("sp", "tp", None),
        P("sp", "tp", None),
        P("sp", "tp", None),
        P("sp", "tp", None),
        P("sp", "tp", None),
        P("tp", None),
        P("tp", None),
        P(),
        P(("sp", "tp"), None),
        P(),
        P(),
        P(("sp", "tp"), None),
        P(("sp", "tp"), None),
        P("sp", None, "tp"),
        P("sp", None, "tp"),
        P("sp", "tp", None),
    )
    return jax.shard_map(
        shards, mesh=mesh, in_specs=placed, out_specs=P(("sp", "tp"), None), check_vma=False
    )
```

profile of v0, /device:TPU:4, one launch (start us, length us, event | category | flops | bytes accessed | tf_op | source)
XLA Modules:
  0.0 1056.2 jit_solution(8099935244267239298)
XLA Ops:
  15.5 68.6 %all-gather.6.cloned.1.call-done = bf16[24576,1,128]{2,0,1:T(8,128)(2,1)} async-done(((bf16[384,1,128]{2,0,1:T(8,128)(2,1)}), bf16[24576,1,128]{2,0,1:T(8,128)(2,1)}) %all-gather.6.cloned.1.call-update) | async-done | bytes 6291472 | tf_op jit(solution)/shard_map/all_gather | solution.py:126
  84.1 21.6 %reshape.640 = bf16[48,512,1,2,64]{4,3,1,0,2:T(2,128)(2,1)} reshape(bf16[24576,1,128]{2,0,1:T(8,128)(2,1)} %all-gather.6.cloned.1.call-done) | data formatting | bytes 12582912 | tf_op jit(solution)/shard_map/reshape | solution.py:45
  105.6 25.9 %copy.98 = bf16[48,512,1,2,64]{1,4,3,2,0:T(8,128)(2,1)} copy(bf16[48,512,1,2,64]{4,3,1,0,2:T(2,128)(2,1)} %reshape.640) | data formatting | bytes 12582912
  131.5 26.5 %all-gather.8.cloned.1.call-done = bf16[24576,1,128]{2,0,1:T(8,128)(2,1)} async-done(((bf16[384,1,128]{2,0,1:T(8,128)(2,1)}), bf16[24576,1,128]{2,0,1:T(8,128)(2,1)}) %all-gather.8.cloned.1.call-update) | async-done | bytes 6291472 | tf_op jit(solution)/shard_map/all_gather | solution.py:127
  158.1 109.4 %while.30 = (s32[]{:T(128)}, f32[1,2,384]{2,1,0:T(2,128)S(1)}, f32[1,2,384]{2,1,0:T(2,128)S(1)}, f32[1,2,384,128]{3,2,1,0:T(8,128)S(1)}, s32[48]{0:T(128)S(1)}, ...) while((s32[]{:T(128)}, f32[1,2,384]{2,1,0:T(2,128)S(1)}, ...), condition=%wide.region_5.6_spmd.clone, body=%wide.region_0.5_spmd.clone.sunk | while | flops 155520128 | bytes 7895871 | solution.py:81
  267.5 18.3 %reshape.641 = bf16[48,512,1,2,128]{4,3,1,0,2:T(2,128)(2,1)} reshape(bf16[24576,1,256]{2,0,1:T(8,128)(2,1)} %all-gather.10.cloned.1.call-done) | data formatting | bytes 25165824 | tf_op jit(solution)/shard_map/reshape | solution.py:45
  285.8 11.5 %copy.101 = bf16[48,512,1,2,128]{4,1,3,2,0:T(8,128)(2,1)} copy(bf16[48,512,1,2,128]{4,3,1,0,2:T(2,128)(2,1)} %reshape.641) | data formatting | bytes 25165824
  297.2 27.9 %all-gather.12.cloned.1.call-done = bf16[24576,1,128]{2,0,1:T(8,128)(2,1)} async-done(((bf16[384,1,128]{2,0,1:T(8,128)(2,1)}), bf16[24576,1,128]{2,0,1:T(8,128)(2,1)}) %all-gather.12.cloned.1.call-update) | async-done | bytes 6291472 | tf_op jit(solution)/shard_map/all_gather | solution.py:129
  325.2 109.3 %while.31 = (s32[]{:T(128)}, f32[1,2,384]{2,1,0:T(2,128)S(1)}, f32[1,2,384]{2,1,0:T(2,128)S(1)}, f32[1,2,384,128]{3,2,1,0:T(8,128)S(1)}, s32[48]{0:T(128)S(1)}, ...) while((s32[]{:T(128)}, f32[1,2,384]{2,1,0:T(2,128)S(1)}, ...), condition=%wide.region_12.13_spmd.clone, body=%wide.region_7.0_spmd.clone.sunk | while | flops 205851776 | bytes 8125247 | solution.py:81
  448.4 6.1 reshape.623
  454.5 411.5 %all_to_all.31 = bf16[64,12,2048]{2,1,0:T(8,128)(2,1)S(1)} all-to-all(bf16[64,12,2048]{2,1,0:T(8,128)(2,1)} %reshape.623), channel_id=1, replica_groups=mesh['sp'=64,'tp'=2] {'sp'}, dimensions={0} | all-to-all | bytes 6291456 | tf_op jit(solution)/shard_map/all_to_all | solution.py:162
  869.4 18.0 %all-gather.14.cloned.1.call-done = bf16[128,12,2048]{2,0,1:T(8,128)(2,1)} async-done(((bf16[64,12,2048]{2,0,1:T(8,128)(2,1)}), bf16[128,12,2048]{2,0,1:T(8,128)(2,1)}) %all-gather.14.cloned.1.call-update) | async-done | bytes 6291472 | tf_op jit(solution)/shard_map/all_gather | solution.py:163
  887.4 9.7 copy.112
  897.0 10.7 %reshape.624 = bf16[1536,2048]{1,0:T(8,128)(2,1)} reshape(bf16[128,12,2048]{2,1,0:T(8,128)(2,1)} %copy.112) | data formatting | bytes 12582912 | tf_op jit(solution)/shard_map/reshape | solution.py:163
  907.7 8.5 fusion.35
  916.2 11.8 %convolution_convert_fusion = bf16[1536,2048]{1,0:T(8,128)(2,1)} fusion(bf16[1,512,2048]{2,1,0:T(8,128)(2,1)S(1)} %copy-done, bf16[1536,2048]{1,0:T(8,128)(2,1)} %reshape.624, f32[1536,512]{1,0:T(8,128)} %fusion.35, bf16[1,2048,512]{2,1,0:T(8,128)(2,1)} %param.40), kind=kOutput, calls=%fused_computation.49 | convolution fusion | flops 6450315264 | bytes 19922944 | tf_op jit(solution)/shard_map/dot_general | solution.py:167
  928.0 15.2 %all_to_all.32 = bf16[2,768,2048]{2,1,0:T(8,128)(2,1)} all-to-all(bf16[2,768,2048]{2,1,0:T(8,128)(2,1)} %bitcast.149), channel_id=1, replica_groups=mesh['sp'=64,'tp'=2] {'tp'}, dimensions={0} | all-to-all | bytes 12582912 | tf_op jit(solution)/shard_map/all_to_all | solution.py:20
  943.3 6.9 reduce_sum.116
  950.1 6.1 reshape.626
  956.2 10.7 %all-to-all-start.3 = ((bf16[64,12,2048]{2,1,0:T(8,128)(2,1)}), bf16[64,12,2048]{2,1,0:T(8,128)(2,1)}, u32[]{:S(2)}, u32[]{:S(2)}) async-start(bf16[64,12,2048]{2,1,0:T(8,128)(2,1)} %reshape.626), calls=%async_computation.3 | async-start | bytes 8388608 | tf_op jit(solution)/shard_map/all_to_all | solution.py:173
  967.5 54.2 %all-to-all-done.3 = bf16[64,12,2048]{2,1,0:T(8,128)(2,1)} async-done(((bf16[64,12,2048]{2,1,0:T(8,128)(2,1)}), bf16[64,12,2048]{2,1,0:T(8,128)(2,1)}, u32[]{:S(2)}, u32[]{:S(2)}) %all-to-all-start.3) | async-done | bytes 3145760 | tf_op jit(solution)/shard_map/all_to_all | solution.py:173
  1021.7 6.2 reshape.627
  1027.9 7.4 gather_fusion
  1039.0 7.8 multiply_reduce_fusion
  (440 shorter events, 147.8 us)
Async XLA Ops:
  6.5 909.6 %copy-start = (bf16[1,512,2048]{2,1,0:T(8,128)(2,1)S(1)}, bf16[1,512,2048]{2,1,0:T(8,128)(2,1)}, u32[]{:S(2)}) copy-start(bf16[1,512,2048]{2,1,0:T(8,128)(2,1)} %param.41) | copy-start | bytes 6291460
  6.5 8.7 copy-start.6
  6.5 5.9 copy-start.4
  6.5 6.0 copy-start.10
  6.5 7.5 copy-start.8
  6.5 8.2 copy-start.9
  6.6 8.9 copy-start.5
  6.6 77.5 %all-gather.6.cloned.1.call-start = ((), (), s32[]{:S(2)}) async-start(), calls=%async_computation.4 | async-start | bytes 6389760 | tf_op jit(solution)/shard_map/all_gather | solution.py:126
  7.3 150.7 %all-gather.8.cloned.1.call-start = ((), (), s32[]{:S(2)}) async-start(), calls=%async_computation.5 | async-start | bytes 6389760 | tf_op jit(solution)/shard_map/all_gather | solution.py:127
  8.1 259.4 %all-gather.10.cloned.1.call-start = ((), (), s32[]{:S(2)}) async-start(), calls=%async_computation.6 | async-start | bytes 12779520 | tf_op jit(solution)/shard_map/all_gather | solution.py:128
  8.8 316.3 %all-gather.12.cloned.1.call-start = ((), (), s32[]{:S(2)}) async-start(), calls=%async_computation.7 | async-start | bytes 6389760 | tf_op jit(solution)/shard_map/all_gather | solution.py:129
  9.4 878.0 %all-gather.14.cloned.1.call-start = ((), (), s32[]{:S(2)}) async-start(), calls=%async_computation.8 | async-start | bytes 9437184 | tf_op jit(solution)/shard_map/all_gather | solution.py:163
  436.3 5.8 copy-start.3
  444.4 1.2 copy-start.1
  956.2 11.1 %copy-start.7 = (f32[192,2]{0,1:T(2,128)S(1)}, f32[192,2]{0,1:T(2,128)}, u32[]{:S(2)}) copy-start(f32[192,2]{0,1:T(2,128)} %param.38) | copy-start | bytes 4612
  956.2 65.5 %all-to-all-start.3 = ((bf16[64,12,2048]{2,1,0:T(8,128)(2,1)}), bf16[64,12,2048]{2,1,0:T(8,128)(2,1)}, u32[]{:S(2)}, u32[]{:S(2)}) async-start(bf16[64,12,2048]{2,1,0:T(8,128)(2,1)} %reshape.626), calls=%async_computation.3 | async-start | bytes 8388608 | tf_op jit(solution)/shard_map/all_to_all | solution.py:173
  1039.0 7.8 copy-start.2
Sparse Core Ops, SparseCore 0:
  10.1 73.8 all-gather.5
  86.8 71.1 all-gather.7
  160.8 90.5 all-gather.9
  253.9 71.1 all-gather.11
  869.5 17.7 all-gather.13
where the time goes:
time: 1070 us; the launch traced here: 1060 us
  blocking collectives  431 us (40%)
  local copies, waits for them, and re-layouts  200 us (19%)
  waiting for transfers between devices  198 us (19%)
  loops' own time  131 us (12%)
  matrix products  42.9 us (4%)
  other arithmetic  29.9 us (3%)
  between operations  13.5 us (1%)
  starting transfers between devices  10.9 us (1%)
    all_to_all x1, blocking collectives, shards(): lax.all_to_all(outgoing, 'sp', split_axis=0, concat_axis=0, tiled=True)  412 us
    another operation x2, loops' own time, advance(): lax.scan(update, carried, (key_blocks, value_blocks, jnp.arange(blocks)))  129 us
    all_gather x1, waiting for transfers between devices, shards(): lax.all_gather(key_small, 'sp', axis=0, tiled=True)  68.6 us
    dynamic_slice x96, local copies, waits for them, and re-layouts, advance(): lax.scan(update, carried, (key_blocks, value_blocks, jnp.arange(blocks)))  62.7 us
    all_to_all x1, waiting for transfers between devices, shards(): lax.all_to_all(summed.reshape(experts, capacity, features), 'sp', split_a...  54.2 us
    unnamed x29, local copies, waits for them, and re-layouts  40.6 us
    reshape x2, local copies, waits for them, and re-layouts, advance(): key_blocks = keyset.reshape(blocks, block_rows, head_count, 2, key_width)  39.8 us
    all_gather x1, waiting for transfers between devices, shards(): lax.all_gather(value_large, 'sp', axis=0, tiled=True)  27.9 us
  transfers between devices with their start and end apart: 6, of which 5 were waited for; matrix products, arithmetic and copies ran while one was open for 12% of the time, Pallas kernels for 0%

commit v1 on v0

v1 whole, which is shorter than its diff:
```python
import math

import jax
import jax.numpy as jnp
from jax import lax
from jax.experimental import pallas as pl
from jax.experimental.pallas import tpu as pltpu
from jax.sharding import Mesh, PartitionSpec as P

residual_gain = 8.0**0.25
epsilon = 1e-05
masked_score = -1e30

LOG2E = 1.4426950408889634


def flash_body(meta, slope, qt, keys, values, out, lse, qs, bias, top, acc, *, chunk, place_count, span, lanes):
    block = pl.program_id(0)
    plane = meta[0]
    place = meta[1]
    width = qt.shape[1]
    half = width // 2
    scale = LOG2E * half ** (-0.5)
    slope_two = slope[0] * LOG2E
    rows = span * chunk
    total = 2 * chunk
    qs[...] = jnp.zeros_like(qs)
    qs[:half, :chunk] = qt[0, :half, :]
    qs[half:, chunk:] = qt[0, half:, :]
    bias[...] = slope_two * lax.broadcasted_iota(jnp.int32, bias.shape, 0).astype(jnp.float32)
    top[...] = jnp.full_like(top, masked_score)
    acc[...] = jnp.zeros_like(acc)
    last_query = (block - plane) * (place_count * chunk) + place * chunk + (chunk - 1)

    def step(number, masked):
        shift = slope_two * (number * rows - last_query).astype(jnp.float32)
        key_block = keys[pl.ds(pl.multiple_of(number * rows, rows), rows), :]
        value_parts = [values[number * span + i] for i in range(span)]
        value_block = jnp.concatenate(value_parts, axis=1) if span > 1 else value_parts[0]
        value_block = jnp.concatenate([value_block, jnp.ones((16, rows), jnp.bfloat16)], axis=0)
        for first in range(0, total, lanes):
            cut = slice(first, first + lanes)
            scores = jnp.dot(key_block, qs[:, cut], preferred_element_type=jnp.float32)
            scores = scores * scale + bias[...]
            if masked:
                lane = lax.broadcasted_iota(jnp.int32, (rows, lanes), 1) + first
                lane = jnp.where(lane >= chunk, lane - chunk, lane)
                key_place = lax.broadcasted_iota(jnp.int32, (rows, lanes), 0) + number * rows
                scores = jnp.where(key_place <= lane + place * chunk, scores, masked_score)
            old = top[:, cut]
            new = jnp.maximum(old, jnp.max(scores, axis=0, keepdims=True) + shift)
            probs = jnp.exp2(scores - (new - shift)).astype(jnp.bfloat16)
            product = jnp.dot(value_block, probs, preferred_element_type=jnp.float32)
            acc[:, cut] = acc[:, cut] * jnp.exp2(old - new) + product
            top[:, cut] = new

    full = jnp.where(block > plane, place_count // span, jnp.where(block == plane, place // span, 0))

    def loop(number, carry):
        step(number, False)
        return carry

    lax.fori_loop(0, full, loop, 0)

    @pl.when(block == plane)
    def _():
        step(place // span, True)

    vsize = acc.shape[0] - 16
    sums = jnp.maximum(acc[vsize : vsize + 1, :], 1e-30)
    mixed = acc[:vsize, :] * (1.0 / sums)
    out[0, :, :vsize] = mixed[:, :chunk].T.astype(jnp.bfloat16)
    out[0, :, vsize:] = mixed[:, chunk:].T.astype(jnp.bfloat16)
    lse[0] = top[...] + jnp.log2(sums)


def flash(meta, slope, qt, keys, values, span=2, lanes=256):
    blocks, width, chunk = qt.shape
    place_count, vsize, _ = values.shape
    rows = span * chunk
    body = lambda *refs: flash_body(*refs, chunk=chunk, place_count=place_count, span=span, lanes=lanes)
    return pl.pallas_call(
        body,
        grid=(blocks,),
        in_specs=[
            pl.BlockSpec(memory_space=pltpu.SMEM),
            pl.BlockSpec(memory_space=pltpu.SMEM),
            pl.BlockSpec((1, width, chunk), lambda b: (b, 0, 0)),
            pl.BlockSpec((place_count * chunk, width), lambda b: (0, 0)),
            pl.BlockSpec((place_count, vsize, chunk), lambda b: (0, 0, 0)),
        ],
        out_specs=[
            pl.BlockSpec((1, chunk, 2 * vsize), lambda b: (b, 0, 0)),
            pl.BlockSpec((1, 1, 2 * chunk), lambda b: (b, 0, 0)),
        ],
        out_shape=[
            jax.ShapeDtypeStruct((blocks, chunk, 2 * vsize), jnp.bfloat16),
            jax.ShapeDtypeStruct((blocks, 1, 2 * chunk), jnp.float32),
        ],
        scratch_shapes=[
            pltpu.VMEM((width, 2 * chunk), jnp.bfloat16),
            pltpu.VMEM((rows, lanes), jnp.float32),
            pltpu.VMEM((1, 2 * chunk), jnp.float32),
            pltpu.VMEM((vsize + 16, 2 * chunk), jnp.float32),
        ],
        compiler_params=pltpu.CompilerParams(
            dimension_semantics=("arbitrary",), vmem_limit_bytes=56 * 1024 * 1024
        ),
    )(meta, slope, qt, keys, values)


def cut_along(shard, dim, size):
    before, after = (shard.shape[:dim], shard.shape[dim + 1 :])
    return jnp.moveaxis(shard.reshape(*before, size, -1, *after), dim, 0)


def sent_and_summed(shard, axis, dim):
    blocks = cut_along(shard, dim, lax.axis_size(axis))
    arrived = lax.all_to_all(blocks, axis, split_axis=0, concat_axis=0, tiled=True)
    return arrived.astype(jnp.float32).sum(axis=0)


def layer_norm(values, gain_row):
    average = jnp.mean(values, axis=-1, keepdims=True)
    centred = values - average
    variance = jnp.mean(centred * centred, axis=-1, keepdims=True)
    return centred * lax.rsqrt(variance + epsilon) * gain_row.astype(jnp.float32)


SP = ("z", "y", "x")
PLANE = ("y", "x")
OWNERS = ("z", "tp")


def exchanged(part_out, part_lse, core_count, value_size):
    planes, length, _ = part_out.shape
    row_count = length // core_count
    sent = part_out.reshape(planes * core_count, row_count, -1)
    arrived = lax.all_to_all(sent, OWNERS, split_axis=0, concat_axis=0, tiled=True)
    levels = part_lse.reshape(planes, 2, core_count, row_count)
    levels = jnp.transpose(levels, (0, 2, 1, 3)).reshape(planes * core_count, 2, row_count)
    levels = lax.all_to_all(levels, OWNERS, split_axis=0, concat_axis=0, tiled=True)
    levels = levels.reshape(planes, core_count, 2, row_count)
    weights = jnp.exp2(levels - jnp.max(levels, axis=0, keepdims=True))
    weights = weights / jnp.sum(weights, axis=0, keepdims=True)
    parts = arrived.reshape(planes, core_count, row_count, 2, value_size).astype(jnp.float32)
    weights = jnp.transpose(weights, (0, 1, 3, 2))[..., None]
    return jnp.sum(weights * parts, axis=0)


def finish(mixture, lambda_column, head_gain):
    head_out = mixture[:, :, 0] - lambda_column[:, None, None] * mixture[:, :, 1]
    scaled = head_out * lax.rsqrt(jnp.mean(head_out * head_out, axis=-1, keepdims=True) + epsilon)
    return scaled * head_gain.astype(jnp.float32)


def shards(
    query_small,
    key_small,
    value_small,
    query_large,
    key_large,
    value_large,
    lambdas,
    slopes,
    head_gain,
    residual,
    out_weight,
    norm_gains,
    routes,
    route_weights,
    gate_weight,
    up_weight,
    down_weight,
):
    length = query_small.shape[0]
    planes = lax.axis_size("z")
    places = lax.axis_size("y") * lax.axis_size("x")
    value_size = value_small.shape[2]
    plane = lax.axis_index("z")
    place = lax.axis_index(PLANE)
    mirror = [(i, planes - 1 - i) for i in range(planes)]
    large_pack = jnp.concatenate([key_large.reshape(length, -1), value_large.reshape(length, -1)], axis=1)
    large_pack = lax.ppermute(large_pack, "z", mirror)
    key_width = key_large.shape[2]
    small_keys = lax.all_gather(key_small.reshape(length, -1), PLANE, axis=0, tiled=True)
    small_values = lax.all_gather(value_small.reshape(length, -1).T, PLANE, axis=0)
    small_queries = lax.all_gather(query_small.reshape(length, -1).T, "z", axis=0)
    large_queries = lax.all_gather(query_large.reshape(length, -1).T, "z", axis=0)
    large_keys = lax.all_gather(large_pack[:, :key_width], PLANE, axis=0, tiled=True)
    large_values = lax.all_gather(large_pack[:, key_width:].T, PLANE, axis=0)
    small_meta = jnp.stack([plane, place]).astype(jnp.int32)
    large_meta = jnp.stack([planes - 1 - plane, place]).astype(jnp.int32)
    small_out, small_lse = flash(small_meta, slopes[0, :1], small_queries, small_keys, small_values)
    large_out, large_lse = flash(large_meta, slopes[0, 1:], large_queries, large_keys, large_values)
    core_count = lax.axis_size("tp")
    row_count = length // core_count
    small_mixed = exchanged(small_out, small_lse, core_count, value_size)
    large_mixed = exchanged(large_out, large_lse, core_count, value_size)
    all_lambdas = lax.all_gather(lambdas[0], "tp", axis=0)
    attended = jnp.stack(
        [
            finish(small_mixed, all_lambdas[:, 0], head_gain),
            finish(large_mixed, all_lambdas[:, 1], head_gain),
        ],
        axis=1,
    ).astype(jnp.bfloat16)
    regrouped = jnp.transpose(attended, (2, 0, 1, 3)).reshape(row_count, -1)
    projected = jnp.dot(regrouped, out_weight, preferred_element_type=jnp.float32)
    middle = layer_norm(
        residual_gain * residual.astype(jnp.float32) + projected, norm_gains[0]
    ).astype(jnp.bfloat16)
    experts = lax.axis_size(SP)
    capacity = 4 * row_count // experts
    features = middle.shape[1]
    chosen = routes.reshape(-1)
    matches = (chosen[:, None] == jnp.arange(experts)[None, :]).astype(jnp.int32)
    earlier = jnp.cumsum(matches, axis=0) - matches
    target = chosen * capacity + jnp.sum(earlier * matches, axis=1)
    selector = jnp.any(
        target.reshape(row_count, 2)[None, :, :] == jnp.arange(experts * capacity)[:, None, None],
        axis=2,
    ).astype(jnp.bfloat16)
    outgoing = jnp.dot(selector, middle, preferred_element_type=jnp.float32).astype(jnp.bfloat16)
    outgoing = outgoing.reshape(experts, capacity, features)
    arrived = lax.all_to_all(outgoing, SP, split_axis=0, concat_axis=0, tiled=True)
    paired = lax.all_gather(arrived, "tp", axis=0, tiled=True).reshape(-1, features)
    gate_in = jnp.dot(paired, gate_weight[0], preferred_element_type=jnp.float32)
    upward = jnp.dot(paired, up_weight[0], preferred_element_type=jnp.float32)
    hidden = (jax.nn.silu(gate_in) * upward).astype(jnp.bfloat16)
    partial_value = jnp.dot(hidden, down_weight[0], preferred_element_type=jnp.float32).astype(
        jnp.bfloat16
    )
    summed = sent_and_summed(
        lax.optimization_barrier(partial_value).astype(jnp.float32).astype(jnp.bfloat16), "tp", 0
    ).astype(jnp.bfloat16)
    returned = lax.all_to_all(
        summed.reshape(experts, capacity, features), SP, split_axis=0, concat_axis=0, tiled=True
    )
    expert_out = returned.reshape(experts * capacity, features)
    picked = jnp.take(expert_out, target, axis=0).reshape(row_count, 2, features)
    moe_sum = jnp.sum(route_weights[:, :, None] * picked.astype(jnp.float32), axis=1)
    return layer_norm(residual_gain * middle.astype(jnp.float32) + moe_sum, norm_gains[1]).astype(
        jnp.bfloat16
    )


def solution(mesh):
    cube = Mesh(mesh.devices.reshape(4, 4, 4, 2), ("z", "y", "x", "tp"))
    both = SP + ("tp",)
    placed = (
        P(SP, "tp", None),
        P(SP, "tp", None),
        P(SP, "tp", None),
        P(SP, "tp", None),
        P(SP, "tp", None),
        P(SP, "tp", None),
        P("tp", None),
        P("tp", None),
        P(),
        P(both, None),
        P(),
        P(),
        P(both, None),
        P(both, None),
        P(SP, None, "tp"),
        P(SP, None, "tp"),
        P(SP, "tp", None),
    )
    return jax.shard_map(
        shards, mesh=cube, in_specs=placed, out_specs=P(both, None), check_vma=False
    )
```

time: 1070 us -> 545 us (0.51)
  blocking collectives: 431 us -> 111 us
  local copies, waits for them, and re-layouts: 200 us -> 63.5 us
  loops' own time: 131 us -> 0 us
  starting transfers between devices: 10.9 us -> 67.8 us
  Pallas kernels: 0 us -> 55.4 us
  waiting for transfers between devices: 198 us -> 169 us
  matrix products: 42.9 us -> 25.6 us
    all_to_all x2 -> x1, blocking collectives: 415 us -> 67.5 us  [shards(): lax.all_to_all(outgoing, SP, split_axis=0, concat_axis=0, tiled=True)]
    another operation x98 -> x0, loops' own time: 131 us -> none  [the longest x2 129 us: advance(): lax.scan(update, carried, (key_blocks, value_blocks, jnp.arange(blocks)))]
    dynamic_slice x96 -> x0, local copies, waits for them, and re-layouts: 62.7 us -> none  [advance(): lax.scan(update, carried, (key_blocks, value_blocks, jnp.arange(blocks)))]
    pallas_call x0 -> x2, Pallas kernels: none -> 55.4 us  [flash(): pl.pallas_call(body, grid=(blocks,), in_specs=[pl.BlockSpec(memory_space=...]
    all_to_all x1 -> x5, starting transfers between devices: 10.7 us -> 63.3 us  [the longest x2 45.5 us: exchanged(): lax.all_to_all(levels, OWNERS, split_axis=0, concat_axis=0, tiled=True)]
    all_gather x4, waiting for transfers between devices: 123 us -> 76.2 us  [the longest x1 43.3 us: shards(): lax.all_gather(key_small.reshape(length, -1), PLANE, axis=0, tiled=True)]
    unnamed x29 -> x26, local copies, waits for them, and re-layouts: 40.6 us -> 1.11 us
    reshape x3 -> x5, local copies, waits for them, and re-layouts: 39.9 us -> 1.49 us  [the longest x4 1.4 us: exchanged(): levels = part_lse.reshape(planes, 2, core_count, row_count)]
  transfers between devices with their start and end apart: 6 -> 11, of which waited for: 5 -> 9; matrix products, arithmetic and copies ran while one was open for 12% -> 5% of each run, Pallas kernels for 0% -> 10%
where the time goes in v1:
time: 545 us; the launch traced here: 535 us
  waiting for transfers between devices  169 us (31%)
  blocking collectives  111 us (20%)
  starting transfers between devices  67.8 us (12%)
  local copies, waits for them, and re-layouts  63.5 us (12%)
  Pallas kernels  55.4 us (10%)
  other arithmetic  28 us (5%)
  matrix products  25.6 us (5%)
  between operations  14 us (3%)
    all_to_all x1, blocking collectives, shards(): lax.all_to_all(outgoing, SP, split_axis=0, concat_axis=0, tiled=True)  67.5 us
    pallas_call x2, Pallas kernels, flash(): pl.pallas_call(body, grid=(blocks,), in_specs=[pl.BlockSpec(memory_space=...  55.4 us
    all_to_all x1, waiting for transfers between devices, shards(): lax.all_to_all(summed.reshape(experts, capacity, features), SP, split_axi...  53.3 us
    all_to_all x2, starting transfers between devices, exchanged(): lax.all_to_all(levels, OWNERS, split_axis=0, concat_axis=0, tiled=True)  45.5 us
    all_gather x1, waiting for transfers between devices, shards(): lax.all_gather(key_small.reshape(length, -1), PLANE, axis=0, tiled=True)  43.3 us
    all_gather x1, waiting for transfers between devices, shards(): lax.all_gather(large_pack[:, :key_width], PLANE, axis=0, tiled=True)  32.3 us
    all_gather x1, waiting for transfers between devices, shards(): lax.all_gather(arrived, 'tp', axis=0, tiled=True).reshape(-1, features)  18.1 us
    all_to_all x1, blocking collectives, sent_and_summed(): lax.all_to_all(blocks, axis, split_axis=0, concat_axis=0, tiled=True)  15.4 us
  transfers between devices with their start and end apart: 11, of which 9 were waited for; matrix products, arithmetic and copies ran while one was open for 5% of the time, Pallas kernels for 10%

profile of v1, /device:TPU:4, one launch (start us, length us, event | category | flops | bytes accessed | tf_op | source)
XLA Modules:
  0.0 534.9 jit_solution(5582688392261023754)
XLA Ops:
  9.1 4.1 collective-permute-start
  13.2 7.0 %collective-permute-done = bf16[384,384]{1,0:T(8,128)(2,1)S(1)} collective-permute-done((bf16[384,384]{1,0:T(8,128)(2,1)S(1)}, bf16[384,384]{1,0:T(8,128)(2,1)S(1)}, u32[]{:S(2)}, u32[]{:S(2)}) %collective-permute-start) | collective-permute-done | bytes 294944 | tf_op jit(solution)/shard_map/ppermute | solution.py:184
  25.4 12.8 %all-gather = bf16[512,384]{0,1:T(8,128)(2,1)S(1)} all-gather(bf16[128,384]{0,1:T(8,128)(2,1)S(1)} %bitcast.128), channel_id=2, replica_groups=mesh['z'=4,'y'=4,'x'=4,'tp'=2] {'z'}, dimensions={0}, use_global_device_ids=true | all-gather | bytes 491520 | tf_op jit(solution)/shard_map/all_gather | solution.py:188
  40.7 13.9 %all-gather.3 = bf16[1024,384]{0,1:T(8,128)(2,1)S(1)} all-gather(bf16[256,384]{0,1:T(8,128)(2,1)S(1)} %bitcast.125), channel_id=5, replica_groups=mesh['z'=4,'y'=4,'x'=4,'tp'=2] {'z'}, dimensions={0}, use_global_device_ids=true | all-gather | bytes 983040 | tf_op jit(solution)/shard_map/all_gather | solution.py:189
  57.7 43.3 %all-gather.16.cloned.1.call-done = bf16[6144,1,128]{2,0,1:T(8,128)(2,1)} async-done(((bf16[384,1,128]{2,0,1:T(8,128)(2,1)}), bf16[6144,1,128]{2,0,1:T(8,128)(2,1)}) %all-gather.16.cloned.1.call-update) | async-done | bytes 1572880 | tf_op jit(solution)/shard_map/all_gather | solution.py:186
  101.0 46.2 %shard_map.163 = (bf16[4,384,256]{2,1,0:T(8,128)(2,1)}, f32[4,1,768]{2,1,0:T(1,128)}) custom-call(s32[2]{0:T(128)} %pad_add_fusion.refs_0_, f32[1]{0:T(128)} %bitcast.2.refs_1_, bf16[4,128,384]{2,1,0:T(8,128)(2,1)} %bitcast.113, bf16[6144,128]{1,0:T(8,128)(2,1)} %bitcast.112, bf16[16,128,384]{2,1,0:T(8,128)(2,1)} %bitcast.102), custom_call_target="tpu_custom_call" | custom-call | tf_op jit(solution)/shard_map/pallas_call | solution.py:82
  163.7 32.3 %all-gather.12.cloned.1.call-done.refs_3_ = bf16[6144,256]{1,0:T(8,128)(2,1)} async-done(((bf16[384,256]{1,0:T(8,128)(2,1)}), bf16[6144,256]{1,0:T(8,128)(2,1)}) %all-gather.12.cloned.1.call-update) | async-done | bytes 3145744 | tf_op jit(solution)/shard_map/all_gather | solution.py:190
  196.0 9.2 %shard_map.164 = (bf16[4,384,256]{2,1,0:T(8,128)(2,1)}, f32[4,1,768]{2,1,0:T(1,128)}) custom-call(s32[2]{0:T(128)} %pad_add_fusion.1.refs_0_, f32[1]{0:T(128)} %bitcast.22.refs_1_, bf16[4,256,384]{2,1,0:T(8,128)(2,1)} %bitcast.103, bf16[6144,256]{1,0:T(8,128)(2,1)} %all-gather.12.cloned.1.call-done.refs_3_, bf16[16,128,384]{2,1,0:T(8,128)(2,1)} %bitcast.101), custom_call_target="tpu_custom_call" | custom-call | tf_op jit(solution)/shard_map/pallas_call | solution.py:82
  206.7 42.1 %all-to-all-start.2 = ((f32[8,2,192]{2,1,0:T(2,128)}), f32[8,2,192]{2,1,0:T(2,128)S(1)}, u32[]{:S(2)}, u32[]{:S(2)}) async-start(f32[8,2,192]{2,1,0:T(2,128)} %bitcast.31), calls=%async_computation.2 | async-start | bytes 32768 | tf_op jit(solution)/shard_map/all_to_all | solution.py:142
  258.0 3.9 multiply_reduce_fusion.4
  263.5 7.4 %all-to-all-done.3 = bf16[8,192,256]{2,1,0:T(8,128)(2,1)S(1)} async-done(((bf16[8,192,256]{2,1,0:T(8,128)(2,1)}), bf16[8,192,256]{2,1,0:T(8,128)(2,1)S(1)}, u32[]{:S(2)}, u32[]{:S(2)}) %all-to-all-start.3) | async-done | bytes 786464 | tf_op jit(solution)/shard_map/all_to_all | solution.py:139
  284.2 6.1 %reshape.253 = bf16[64,12,2048]{2,1,0:T(8,128)(2,1)} reshape(bf16[768,2048]{1,0:T(8,128)(2,1)} %convolution_convert_fusion.1) | data formatting | bytes 6291456 | tf_op jit(solution)/shard_map/reshape | solution.py:225
  290.3 67.5 %all_to_all.35 = bf16[64,12,2048]{2,1,0:T(8,128)(2,1)S(1)} all-to-all(bf16[64,12,2048]{2,1,0:T(8,128)(2,1)} %reshape.253), channel_id=1, replica_groups=mesh['z'=4,'y'=4,'x'=4,'tp'=2] {'z','y','x'}, dimensions={0} | all-to-all | bytes 6291456 | tf_op jit(solution)/shard_map/all_to_all | solution.py:226
  361.3 18.1 %all-gather.14.cloned.1.call-done = bf16[128,12,2048]{2,0,1:T(8,128)(2,1)} async-done(((bf16[64,12,2048]{2,0,1:T(8,128)(2,1)}), bf16[128,12,2048]{2,0,1:T(8,128)(2,1)}) %all-gather.14.cloned.1.call-update) | async-done | bytes 6291472 | tf_op jit(solution)/shard_map/all_gather | solution.py:227
  379.4 9.7 %copy.99 = bf16[128,12,2048]{2,1,0:T(8,128)(2,1)} copy(bf16[128,12,2048]{2,0,1:T(8,128)(2,1)} %all-gather.14.cloned.1.call-done) | data formatting | bytes 12582912 | tf_op jit(solution)/shard_map/all_gather | solution.py:227
  389.1 10.7 %reshape.254 = bf16[1536,2048]{1,0:T(8,128)(2,1)} reshape(bf16[128,12,2048]{2,1,0:T(8,128)(2,1)} %copy.99) | data formatting | bytes 12582912 | tf_op jit(solution)/shard_map/reshape | solution.py:227
  399.8 8.5 %fusion.3 = f32[1536,512]{1,0:T(8,128)} fusion(bf16[1536,2048]{1,0:T(8,128)(2,1)} %reshape.254, bf16[1,2048,512]{2,1,0:T(8,128)(2,1)} %param.31), kind=kOutput, calls=%fused_computation.10 | convolution fusion | flops 3221225472 | bytes 11534336 | tf_op jit(solution)/shard_map/dot_general | solution.py:228
  408.3 11.8 %convolution_convert_fusion = bf16[1536,2048]{1,0:T(8,128)(2,1)} fusion(bf16[1,512,2048]{2,1,0:T(8,128)(2,1)S(1)} %copy-done, bf16[1536,2048]{1,0:T(8,128)(2,1)} %reshape.254, f32[1536,512]{1,0:T(8,128)} %fusion.3, bf16[1,2048,512]{2,1,0:T(8,128)(2,1)} %param.32), kind=kOutput, calls=%fused_computation.1 | convolution fusion | flops 6450315264 | bytes 19922944 | tf_op jit(solution)/shard_map/dot_general | solution.py:231
  420.1 15.4 %all_to_all.36 = bf16[2,768,2048]{2,1,0:T(8,128)(2,1)} all-to-all(bf16[2,768,2048]{2,1,0:T(8,128)(2,1)} %bitcast.100), channel_id=1, replica_groups=mesh['z'=4,'y'=4,'x'=4,'tp'=2] {'tp'}, dimensions={0} | all-to-all | bytes 12582912 | tf_op jit(solution)/shard_map/all_to_all | solution.py:119
  435.5 5.3 reduce_sum.134
  443.6 10.7 %all-to-all-start.6 = ((bf16[64,12,2048]{2,1,0:T(8,128)(2,1)}), bf16[64,12,2048]{2,1,0:T(8,128)(2,1)}, u32[]{:S(2)}, u32[]{:S(2)}) async-start(bf16[64,12,2048]{2,1,0:T(8,128)(2,1)} %reshape.256), calls=%async_computation.6 | async-start | bytes 8388608 | tf_op jit(solution)/shard_map/all_to_all | solution.py:237
  454.9 53.3 %all-to-all-done.6 = bf16[64,12,2048]{2,1,0:T(8,128)(2,1)} async-done(((bf16[64,12,2048]{2,1,0:T(8,128)(2,1)}), bf16[64,12,2048]{2,1,0:T(8,128)(2,1)}, u32[]{:S(2)}, u32[]{:S(2)}) %all-to-all-start.6) | async-done | bytes 3145760 | tf_op jit(solution)/shard_map/all_to_all | solution.py:237
  508.2 4.7 reshape.257
  518.9 6.1 %multiply_reduce_fusion = f32[192,2048]{1,0:T(8,128)S(1)} fusion(bf16[192,2,2048]{2,1,0:T(2,128)(2,1)S(1)} %gather.7, pred[192,2]{1,0:T(8,128)(4,1)S(1)} %copy.97, f32[192,2]{1,0:T(8,128)S(1)} %copy.92), kind=kLoop, calls=%fused_computation.4 | loop fusion | flops 2752512 | bytes 3147648 | tf_op jit(solution)/shard_map/reduce_sum | solution.py:242
  (115 shorter events, 70.7 us)
Async XLA Ops:
  6.5 401.8 %copy-start = (bf16[1,512,2048]{2,1,0:T(8,128)(2,1)S(1)}, bf16[1,512,2048]{2,1,0:T(8,128)(2,1)}, u32[]{:S(2)}) copy-start(bf16[1,512,2048]{2,1,0:T(8,128)(2,1)} %param.33) | copy-start | bytes 6291460
  6.5 15.1 %copy-start.10 = (f32[1,2]{1,0:T(1,128)S(1)}, f32[1,2]{1,0:T(1,128)}, u32[]{:S(2)}) copy-start(f32[1,2]{1,0:T(1,128)} %param.23) | copy-start | bytes 28
  6.5 16.9 %copy-start.7 = (s32[192,2]{0,1:T(2,128)S(1)}, s32[192,2]{0,1:T(2,128)}, u32[]{:S(2)}) copy-start(s32[192,2]{0,1:T(2,128)} %param.29) | copy-start | bytes 4612
  6.5 18.9 %copy-start.5 = (bf16[384,1,128]{2,0,1:T(8,128)(2,1)S(1)}, bf16[384,1,128]{2,0,1:T(8,128)(2,1)}, u32[]{:S(2)}) copy-start(bf16[384,1,128]{2,0,1:T(8,128)(2,1)} %param.17) | copy-start | bytes 294916
  6.5 48.5 %all-gather.18.cloned.1.call-start = ((), (), s32[]{:S(2)}) async-start(), calls=%async_computation.10 | async-start | bytes 1671168 | tf_op jit(solution)/shard_map/all_gather | solution.py:187
  7.3 93.7 %all-gather.16.cloned.1.call-start = ((), (), s32[]{:S(2)}) async-start(), calls=%async_computation.9 | async-start | bytes 1671168 | tf_op jit(solution)/shard_map/all_gather | solution.py:186
  8.0 153.1 %all-gather.20.cloned.1.call-start = ((), (), s32[]{:S(2)}) async-start(), calls=%async_computation.11 | async-start | bytes 1671168 | tf_op jit(solution)/shard_map/all_gather | solution.py:191
  9.1 30.8 %copy-start.9 = (f32[1,2]{1,0:T(1,128)S(1)}, f32[1,2]{1,0:T(1,128)}, u32[]{:S(2)}) copy-start(f32[1,2]{1,0:T(1,128)} %param.24) | copy-start | bytes 28
  9.1 31.6 %copy-start.4 = (bf16[384,1,256]{2,0,1:T(8,128)(2,1)S(1)}, bf16[384,1,256]{2,0,1:T(8,128)(2,1)}, u32[]{:S(2)}) copy-start(bf16[384,1,256]{2,0,1:T(8,128)(2,1)} %param.20) | copy-start | bytes 589828
  9.1 11.1 %collective-permute-start = (bf16[384,384]{1,0:T(8,128)(2,1)S(1)}, bf16[384,384]{1,0:T(8,128)(2,1)S(1)}, u32[]{:S(2)}, u32[]{:S(2)}) collective-permute-start(bf16[384,384]{1,0:T(8,128)(2,1)S(1)} %pad_maximum_fusion), channel_id=1, source_target_pairs={{0,96},{32,64},{64,32},{96,0},{1,97},{33,65},{65,33},{97,1},{2,98}... | collective-permute-start | bytes 884744 | tf_op jit(solution)/shard_map/ppermute | solution.py:184
  20.9 175.2 %all-gather.12.cloned.1.call-start = ((), (), s32[]{:S(2)}) async-start(), calls=%async_computation.7 | async-start | bytes 3342336 | tf_op jit(solution)/shard_map/all_gather | solution.py:190
  101.0 51.6 %copy-start.11 = (bf16[128]{0:T(256)(128)(2,1)S(1)}, bf16[128]{0:T(256)(128)(2,1)}, u32[]{:S(2)}) copy-start(bf16[128]{0:T(256)(128)(2,1)} %param.25) | copy-start | bytes 772
  148.6 8.6 %all-to-all-start = ((f32[8,2,192]{2,1,0:T(2,128)}), f32[8,2,192]{2,1,0:T(2,128)S(1)}, u32[]{:S(2)}, u32[]{:S(2)}) async-start(f32[8,2,192]{2,1,0:T(2,128)} %bitcast.11), calls=%async_computation | async-start | bytes 32768 | tf_op jit(solution)/shard_map/all_to_all | solution.py:142
  152.5 8.5 %copy-start.6 = (bf16[2,2048]{1,0:T(2,128)(2,1)S(1)}, bf16[2,2048]{1,0:T(2,128)(2,1)}, u32[]{:S(2)}) copy-start(bf16[2,2048]{1,0:T(2,128)(2,1)} %param.28) | copy-start | bytes 24580
  157.3 49.5 %all-to-all-start.1 = ((bf16[8,192,256]{2,1,0:T(8,128)(2,1)}), bf16[8,192,256]{2,1,0:T(8,128)(2,1)S(1)}, u32[]{:S(2)}, u32[]{:S(2)}) async-start(bf16[8,192,256]{2,1,0:T(8,128)(2,1)} %bitcast.114), calls=%async_computation.1 | async-start | bytes 1572864 | tf_op jit(solution)/shard_map/all_to_all | solution.py:139
  206.7 47.5 %all-to-all-start.2 = ((f32[8,2,192]{2,1,0:T(2,128)}), f32[8,2,192]{2,1,0:T(2,128)S(1)}, u32[]{:S(2)}, u32[]{:S(2)}) async-start(f32[8,2,192]{2,1,0:T(2,128)} %bitcast.31), calls=%async_computation.2 | async-start | bytes 32768 | tf_op jit(solution)/shard_map/all_to_all | solution.py:142
  254.2 16.6 %all-to-all-start.3 = ((bf16[8,192,256]{2,1,0:T(8,128)(2,1)}), bf16[8,192,256]{2,1,0:T(8,128)(2,1)S(1)}, u32[]{:S(2)}, u32[]{:S(2)}) async-start(bf16[8,192,256]{2,1,0:T(8,128)(2,1)} %bitcast.115), calls=%async_computation.3 | async-start | bytes 1572864 | tf_op jit(solution)/shard_map/all_to_all | solution.py:139
  257.8 121.7 %all-gather.14.cloned.1.call-start = ((), (), s32[]{:S(2)}) async-start(), calls=%async_computation.8 | async-start | bytes 9437184 | tf_op jit(solution)/shard_map/all_gather | solution.py:227
  280.2 1.2 copy-start.2
  443.6 11.2 %copy-start.8 = (f32[192,2]{0,1:T(2,128)S(1)}, f32[192,2]{0,1:T(2,128)}, u32[]{:S(2)}) copy-start(f32[192,2]{0,1:T(2,128)} %param.30) | copy-start | bytes 4612
  443.6 64.7 %all-to-all-start.6 = ((bf16[64,12,2048]{2,1,0:T(8,128)(2,1)}), bf16[64,12,2048]{2,1,0:T(8,128)(2,1)}, u32[]{:S(2)}, u32[]{:S(2)}) async-start(bf16[64,12,2048]{2,1,0:T(8,128)(2,1)} %reshape.256), calls=%async_computation.6 | async-start | bytes 8388608 | tf_op jit(solution)/shard_map/all_to_all | solution.py:237
  518.9 6.1 %copy-start.3 = (f32[192,2048]{1,0:T(8,128)S(1)}, f32[192,2048]{1,0:T(8,128)}, u32[]{:S(2)}) copy-start(f32[192,2048]{1,0:T(8,128)} %copy-done.2) | copy-start | bytes 4718596
  526.1 1.8 copy-start.1
Sparse Core Ops, SparseCore 0:
  9.5 45.5 all-gather.17
  57.2 43.7 all-gather.15
  103.1 43.5 all-gather.19
  148.6 47.3 all-gather.11
  361.5 17.9 all-gather.13

commit v2 on v1

v2 whole, which is shorter than its diff:
```python
import jax
import jax.numpy as jnp
from jax import lax
from jax.experimental import pallas as pl
from jax.experimental.pallas import tpu as pltpu
from jax.sharding import Mesh, PartitionSpec as P

residual_gain = 8.0**0.25
epsilon = 1e-05
masked_score = -1e30
LOG2E = 1.4426950408889634
SP = ("z", "y", "x")
PLANE = ("y", "x")
OWNERS = ("z", "tp")
SPAN = 2
LANES = 256
VMEM_LIMIT = 56 * 1024 * 1024


def three_parts(value):
    high = value.astype(jnp.bfloat16).astype(jnp.float32)
    rest = value - high
    middle = rest.astype(jnp.bfloat16).astype(jnp.float32)
    return high, middle, (rest - middle).astype(jnp.bfloat16).astype(jnp.float32)


def flash_group(plane, place, slope, qt, keys, values, qs, bias, top, acc, sbuf, mbuf):
    block = pl.program_id(0)
    place_count, chunk, width = keys.shape
    half = width // 2
    scale = LOG2E * half ** (-0.5)
    slope_two = slope * LOG2E
    rows = SPAN * chunk
    total = 2 * chunk
    qs[:width, :] = jnp.zeros((width, total), jnp.bfloat16)
    qs[:half, :chunk] = qt[0, :half, :]
    qs[half:width, chunk:] = qt[0, half:, :]
    bias[...] = slope_two * lax.broadcasted_iota(jnp.int32, bias.shape, 0).astype(jnp.float32)
    top[...] = jnp.full_like(top, masked_score)
    acc[...] = jnp.zeros_like(acc)
    last_query = (block - plane) * (place_count * chunk) + place * chunk + (chunk - 1)
    cuts = [slice(first, first + LANES) for first in range(0, total, LANES)]

    def fill(number, slot):
        key_block = keys[pl.ds(number * SPAN, SPAN)].reshape(rows, width)
        for cut in cuts:
            scores = jnp.dot(key_block, qs[:width, cut], preferred_element_type=jnp.float32)
            scores = scores * scale + bias[...]
            sbuf[slot, :, cut] = scores
            mbuf[slot, :, cut] = jnp.max(scores, axis=0, keepdims=True)

    def use(number, slot):
        shift = slope_two * (number * rows - last_query).astype(jnp.float32)
        value_block = jnp.concatenate([values[number * SPAN + i] for i in range(SPAN)], axis=1)
        value_block = jnp.concatenate([value_block, jnp.ones((16, rows), jnp.bfloat16)], axis=0)
        for cut in cuts:
            old = top[:, cut]
            new = jnp.maximum(old, mbuf[slot, :, cut] + shift)
            probs = jnp.exp2(sbuf[slot, :, cut] - (new - shift)).astype(jnp.bfloat16)
            top[:, cut] = new
            product = jnp.dot(value_block, probs, preferred_element_type=jnp.float32)
            acc[:, cut] = acc[:, cut] * jnp.exp2(old - new) + product

    def hide_later_keys(number, slot):
        for cut in cuts:
            lane = lax.broadcasted_iota(jnp.int32, (rows, LANES), 1) + cut.start
            lane = jnp.where(lane >= chunk, lane - chunk, lane)
            key_place = lax.broadcasted_iota(jnp.int32, (rows, LANES), 0) + number * rows
            scores = jnp.where(key_place <= lane + place * chunk, sbuf[slot, :, cut], masked_score)
            sbuf[slot, :, cut] = scores
            mbuf[slot, :, cut] = jnp.max(scores, axis=0, keepdims=True)

    most = place_count // SPAN
    count = jnp.where(block > plane, most, jnp.where(block == plane, place // SPAN + 1, 0))

    @pl.when(count > 0)
    def _():
        fill(0, 0)
        last = count - 1

        def pair_step(pair, carry):
            fill(2 * pair + 1, 1)
            use(2 * pair, 0)
            fill(jnp.minimum(2 * pair + 2, most - 1), 0)
            use(2 * pair + 1, 1)
            return carry

        lax.fori_loop(0, last // 2, pair_step, 0)

        @pl.when(last % 2 == 1)
        def _():
            fill(last, 1)
            use(last - 1, 0)

            @pl.when(block == plane)
            def _():
                hide_later_keys(last, 1)

            use(last, 1)

        @pl.when(last % 2 == 0)
        def _():
            @pl.when(block == plane)
            def _():
                hide_later_keys(last, 0)

            use(last, 0)


def flash_body(
    meta, slopes, lambdas, small_q, large_q, small_k, large_k, small_v, large_v,
    out, qs, bias, top, acc, sbuf, mbuf, tail,
):
    chunk = small_q.shape[2]
    vsize = small_v.shape[1]
    tail[...] = jnp.zeros_like(tail)
    groups = (
        (meta[0], small_q, small_k, small_v),
        (meta[2], large_q, large_k, large_v),
    )
    for number, (plane, qt, keys, values) in enumerate(groups):
        flash_group(
            plane, meta[1], slopes[number], qt, keys, values, qs, bias, top, acc, sbuf, mbuf
        )
        sums = jnp.maximum(acc[vsize : vsize + 1, :], 1e-30)
        mixed = acc[:vsize, :] * (1.0 / sums)
        level = top[...] + jnp.log2(sums)
        lam = jnp.full((1, chunk), lambdas[number], jnp.float32)
        for j in range(2):
            column = (2 * number + j) * vsize
            out[0, :, column : column + vsize] = (
                mixed[:, j * chunk : (j + 1) * chunk].T.astype(jnp.bfloat16)
            )
            for k, part in enumerate(three_parts(level[:, j * chunk : (j + 1) * chunk])):
                row = 6 * k + 2 * number + j
                tail[row : row + 1, :] = part
        for k, part in enumerate(three_parts(lam)):
            row = 6 * k + 4 + number
            tail[row : row + 1, :] = part
    out[0, :, 4 * vsize :] = tail[...].T.astype(jnp.bfloat16)


def flash(meta, slopes, lambdas, small_q, large_q, gathered):
    blocks, small_width, chunk = small_q.shape
    large_width = large_q.shape[1]
    place_count, _, _ = gathered.shape
    vsize = 128
    rows = SPAN * chunk
    scalar = pl.BlockSpec(memory_space=pltpu.SMEM)
    return pl.pallas_call(
        flash_body,
        grid=(blocks,),
        in_specs=[
            scalar,
            scalar,
            scalar,
            pl.BlockSpec((1, small_width, chunk), lambda b: (b, 0, 0)),
            pl.BlockSpec((1, large_width, chunk), lambda b: (b, 0, 0)),
            pl.BlockSpec((place_count, chunk, small_width), lambda b: (0, 0, 2)),
            pl.BlockSpec((place_count, chunk, large_width), lambda b: (0, 0, 0)),
            pl.BlockSpec((place_count, vsize, chunk), lambda b: (0, 3, 0)),
            pl.BlockSpec((place_count, vsize, chunk), lambda b: (0, 4, 0)),
        ],
        out_specs=pl.BlockSpec((1, chunk, 5 * vsize), lambda b: (b, 0, 0)),
        out_shape=jax.ShapeDtypeStruct((blocks, chunk, 5 * vsize), jnp.bfloat16),
        scratch_shapes=[
            pltpu.VMEM((large_width, 2 * chunk), jnp.bfloat16),
            pltpu.VMEM((rows, LANES), jnp.float32),
            pltpu.VMEM((1, 2 * chunk), jnp.float32),
            pltpu.VMEM((vsize + 16, 2 * chunk), jnp.float32),
            pltpu.VMEM((2, rows, 2 * chunk), jnp.float32),
            pltpu.VMEM((2, 1, 2 * chunk), jnp.float32),
            pltpu.VMEM((vsize, chunk), jnp.float32),
        ],
        compiler_params=pltpu.CompilerParams(
            dimension_semantics=("arbitrary",), vmem_limit_bytes=VMEM_LIMIT
        ),
    )(meta, slopes, lambdas, small_q, large_q, gathered, gathered, gathered, gathered)


def normed(values, gain_row):
    average = jnp.mean(values, axis=-1, keepdims=True)
    centred = values - average
    variance = jnp.mean(centred * centred, axis=-1, keepdims=True)
    return centred * lax.rsqrt(variance + epsilon) * gain_row


def merge_body(core, arrived, head_gain, residual, weight, norm_gain, middle, keep, give):
    planes = arrived.shape[0] // 2
    vsize = head_gain.shape[1]
    gain = head_gain[...].astype(jnp.float32)
    pieces = []
    for head in range(2):
        tails = []
        for z in range(planes):
            lanes = arrived[2 * z + head, :, 4 * vsize :].astype(jnp.float32)
            tails.append([lanes[:, i : i + 1] + lanes[:, i + 6 : i + 7] + lanes[:, i + 12 : i + 13] for i in range(6)])
        for group in range(2):
            mixtures = []
            for j in range(2):
                index = 2 * group + j
                highest = tails[0][index]
                for z in range(1, planes):
                    highest = jnp.maximum(highest, tails[z][index])
                weights = [jnp.exp2(tails[z][index] - highest) for z in range(planes)]
                scaled = 1.0 / sum(weights)
                column = index * vsize
                mixtures.append(
                    sum(
                        (weights[z] * scaled)
                        * arrived[2 * z + head, :, column : column + vsize].astype(jnp.float32)
                        for z in range(planes)
                    )
                )
            head_out = mixtures[0] - tails[0][4 + group] * mixtures[1]
            power = jnp.mean(head_out * head_out, axis=-1, keepdims=True)
            pieces.append((head_out * lax.rsqrt(power + epsilon) * gain).astype(jnp.bfloat16))
    attended = jnp.concatenate(pieces, axis=1)
    projected = jnp.dot(attended, weight[...], preferred_element_type=jnp.float32)
    values = residual_gain * residual[...].astype(jnp.float32) + projected
    result = normed(values, norm_gain[...].astype(jnp.float32)).astype(jnp.bfloat16)
    middle[...] = result
    half = result.shape[1] // 2

    @pl.when(core[0] == 0)
    def _():
        keep[...] = result[:, :half]
        give[...] = result[:, half:]

    @pl.when(core[0] == 1)
    def _():
        keep[...] = result[:, half:]
        give[...] = result[:, :half]


def merge(core, arrived, head_gain, residual, weight, norm_gain):
    count, features = residual.shape
    return pl.pallas_call(
        merge_body,
        in_specs=[pl.BlockSpec(memory_space=pltpu.SMEM)] + [pl.BlockSpec(memory_space=pltpu.VMEM)] * 5,
        out_shape=[
            jax.ShapeDtypeStruct((count, features), jnp.bfloat16),
            jax.ShapeDtypeStruct((count, features // 2), jnp.bfloat16),
            jax.ShapeDtypeStruct((count, features // 2), jnp.bfloat16),
        ],
        compiler_params=pltpu.CompilerParams(vmem_limit_bytes=VMEM_LIMIT),
    )(core, arrived, head_gain, residual, weight, norm_gain)


def expert_body(core, mine, other, gate, up, down, keep, give):
    half = mine.shape[1]
    first = pl.multiple_of(core[0] * half, half)
    second = pl.multiple_of((1 - core[0]) * half, half)
    own_rows = mine[...]
    other_rows = other[...]

    def through(weight):
        return jnp.dot(
            own_rows, weight[0, pl.ds(first, half), :], preferred_element_type=jnp.float32
        ) + jnp.dot(
            other_rows, weight[0, pl.ds(second, half), :], preferred_element_type=jnp.float32
        )

    gate_in = through(gate)
    upward = through(up)
    hidden = (gate_in * (1.0 / (1.0 + jnp.exp(-gate_in))) * upward).astype(jnp.bfloat16)
    keep[...] = jnp.dot(
        hidden, down[0, :, pl.ds(first, half)], preferred_element_type=jnp.float32
    ).astype(jnp.bfloat16)
    give[...] = jnp.dot(
        hidden, down[0, :, pl.ds(second, half)], preferred_element_type=jnp.float32
    ).astype(jnp.bfloat16)


def expert(core, mine, other, gate, up, down):
    count, half = mine.shape
    block_rows = 256
    rows = pl.BlockSpec((block_rows, half), lambda i: (i, 0))
    shape = jax.ShapeDtypeStruct((count, half), jnp.bfloat16)
    return pl.pallas_call(
        expert_body,
        grid=(count // block_rows,),
        in_specs=[
            pl.BlockSpec(memory_space=pltpu.SMEM),
            rows,
            rows,
            pl.BlockSpec(gate.shape, lambda i: (0, 0, 0)),
            pl.BlockSpec(up.shape, lambda i: (0, 0, 0)),
            pl.BlockSpec(down.shape, lambda i: (0, 0, 0)),
        ],
        out_specs=[rows, rows],
        out_shape=[shape, shape],
        compiler_params=pltpu.CompilerParams(
            dimension_semantics=("arbitrary",), vmem_limit_bytes=VMEM_LIMIT
        ),
    )(core, mine, other, gate, up, down)


def final_body(core, own, received, middle, norm_gain, out, total):
    half = own.shape[1]

    @pl.when(core[0] == 0)
    def _():
        total[:, :half] = own[...]
        total[:, half:] = received[...]

    @pl.when(core[0] == 1)
    def _():
        total[:, :half] = received[...]
        total[:, half:] = own[...]

    values = residual_gain * middle[...].astype(jnp.float32) + total[...]
    out[...] = normed(values, norm_gain[...].astype(jnp.float32)).astype(jnp.bfloat16)


def final(core, own, received, middle, norm_gain):
    return pl.pallas_call(
        final_body,
        in_specs=[pl.BlockSpec(memory_space=pltpu.SMEM)] + [pl.BlockSpec(memory_space=pltpu.VMEM)] * 4,
        out_shape=jax.ShapeDtypeStruct(middle.shape, jnp.bfloat16),
        scratch_shapes=[pltpu.VMEM(middle.shape, jnp.float32)],
        compiler_params=pltpu.CompilerParams(vmem_limit_bytes=VMEM_LIMIT),
    )(core, own, received, middle, norm_gain)


def slots(routes, experts, block, offset):
    chosen = routes.reshape(-1)
    matches = (chosen[:, None] == jnp.arange(experts)[None, :]).astype(jnp.int32)
    earlier = jnp.cumsum(matches, axis=0) - matches
    rank = jnp.sum(earlier * matches, axis=1)
    return (chosen * block + offset + rank).reshape(routes.shape)


def shards(
    query_small,
    key_small,
    value_small,
    query_large,
    key_large,
    value_large,
    lambdas,
    slopes,
    head_gain,
    residual,
    out_weight,
    norm_gains,
    routes,
    route_weights,
    gate_weight,
    up_weight,
    down_weight,
):
    length = query_small.shape[0]
    planes = lax.axis_size("z")
    plane = lax.axis_index("z")
    place = lax.axis_index(PLANE)
    core = lax.axis_index("tp")
    mirror = [(i, planes - 1 - i) for i in range(planes)]
    swap = [(0, 1), (1, 0)]
    key_width = key_large.shape[2]
    large_pack = jnp.concatenate(
        [key_large.reshape(length, -1), value_large.reshape(length, -1)], axis=1
    )
    large_pack = lax.ppermute(large_pack, "z", mirror)
    packed = jnp.concatenate(
        [
            jnp.concatenate([large_pack[:, :key_width], key_small.reshape(length, -1)], axis=1),
            value_small.reshape(length, -1).T,
            large_pack[:, key_width:].T,
        ],
        axis=0,
    )
    gathered = lax.all_gather(packed, PLANE, axis=0)
    small_queries = lax.all_gather(query_small.reshape(length, -1).T, "z", axis=0)
    large_queries = lax.all_gather(query_large.reshape(length, -1).T, "z", axis=0)

    core_count = lax.axis_size("tp")
    row_count = length // core_count
    experts = lax.axis_size(SP)
    block = core_count * (4 * row_count // experts)
    their_routes = lax.ppermute(routes, "tp", swap)
    their_weights = lax.ppermute(route_weights, "tp", swap)
    capacity = block // core_count
    target = jnp.concatenate(
        [
            slots(routes, experts, block, core * capacity),
            slots(their_routes, experts, block, (1 - core) * capacity),
        ],
        axis=0,
    )
    shares = jnp.concatenate([route_weights, their_weights], axis=0)
    places = jnp.arange(experts * block)
    hits = [target[:, k] for k in range(2)]
    selector = (
        (hits[0][None, :] == places[:, None]) | (hits[1][None, :] == places[:, None])
    ).astype(jnp.bfloat16)
    spread = jnp.where(hits[0][:, None] == places[None, :], shares[:, :1], 0.0) + jnp.where(
        hits[1][:, None] == places[None, :], shares[:, 1:], 0.0
    )
    spread_top = lax.reduce_precision(spread, exponent_bits=8, mantissa_bits=7)
    spread_high = spread_top.astype(jnp.bfloat16)
    spread_low = (spread - spread_top).astype(jnp.bfloat16)

    meta = jnp.stack([plane, place, planes - 1 - plane]).astype(jnp.int32)
    parts = flash(meta, slopes[0], lambdas[0], small_queries, large_queries, gathered)
    parts = parts.reshape(planes * core_count, row_count, -1)
    parts = lax.all_to_all(parts, OWNERS, split_axis=0, concat_axis=0, tiled=True)
    which = core.astype(jnp.int32).reshape(1)
    middle, keep, give = merge(
        which, parts, head_gain.reshape(1, -1), residual, out_weight, norm_gains[:1]
    )
    half = keep.shape[1]
    tokens = jnp.concatenate([keep, lax.ppermute(give, "tp", swap)], axis=0)
    outgoing = jnp.dot(selector, tokens, preferred_element_type=jnp.float32).astype(jnp.bfloat16)
    arrived = lax.all_to_all(
        outgoing.reshape(experts, block, half), SP, split_axis=0, concat_axis=0, tiled=True
    ).reshape(experts * block, half)
    sides = 2
    side_rows = experts * block // sides
    mine = [arrived[i * side_rows : (i + 1) * side_rows] for i in range(sides)]
    other = [lax.ppermute(rows, "tp", swap) for rows in mine]
    summed = []
    for i in range(sides):
        kept, given = expert(which, mine[i], other[i], gate_weight, up_weight, down_weight)
        got = lax.ppermute(given, "tp", swap)
        summed.append((kept.astype(jnp.float32) + got.astype(jnp.float32)).astype(jnp.bfloat16))
    returned = lax.all_to_all(
        jnp.concatenate(summed, axis=0).reshape(experts, block, half),
        SP,
        split_axis=0,
        concat_axis=0,
        tiled=True,
    ).reshape(experts * block, half)

    def weighed(first):
        cut = slice(first, first + row_count)
        return jnp.dot(spread_high[cut], returned, preferred_element_type=jnp.float32) + jnp.dot(
            spread_low[cut], returned, preferred_element_type=jnp.float32
        )

    received = lax.ppermute(weighed(row_count), "tp", swap)
    return final(which, weighed(0), received, middle, norm_gains[1:])


def solution(mesh):
    cube = Mesh(mesh.devices.reshape(4, 4, 4, 2), ("z", "y", "x", "tp"))
    both = SP + ("tp",)
    placed = (
        P(SP, "tp", None),
        P(SP, "tp", None),
        P(SP, "tp", None),
        P(SP, "tp", None),
        P(SP, "tp", None),
        P(SP, "tp", None),
        P("tp", None),
        P("tp", None),
        P(),
        P(both, None),
        P(),
        P(),
        P(both, None),
        P(both, None),
        P(SP, None, "tp"),
        P(SP, None, "tp"),
        P(SP, "tp", None),
    )
    return jax.shard_map(
        shards, mesh=cube, in_specs=placed, out_specs=P(both, None), check_vma=False
    )
```

time: 545 us -> 317 us (0.58); the launches traced: 535 us -> 315 us
  waiting for transfers between devices: 169 us -> 114 us
  local copies, waits for them, and re-layouts: 63.5 us -> 10.8 us
  starting transfers between devices: 67.8 us -> 18.4 us
  blocking collectives: 111 us -> 81.1 us
  matrix products: 25.6 us -> 8.14 us
  other arithmetic: 28 us -> 11.2 us
    all_gather x5 -> x1, waiting for transfers between devices: 94.3 us -> 40.7 us  [shards(): gathered = lax.all_gather(packed, PLANE, axis=0)]
    all_to_all x5 -> x2, starting transfers between devices: 63.3 us -> 12.4 us  [the longest x1 7.05 us: shards(): lax.all_to_all(jnp.concatenate(summed, axis=0).reshape(experts, block, ha...]
    all_to_all x2 -> x1, blocking collectives: 82.9 us -> 54.7 us  [shards(): lax.all_to_all(outgoing.reshape(experts, block, half), SP, split_axis=0,...]
    reshape x10 -> x0, local copies, waits for them, and re-layouts: 25.9 us -> none  [the longest x1 10.7 us: shards(): lax.all_gather(arrived, 'tp', axis=0, tiled=True).reshape(-1, features)]
    reduce_sum x11 -> x2, other arithmetic: 20.9 us -> 0.23 us  [slots(): rank = jnp.sum(earlier * matches, axis=1)]
    dot_general x4 -> x5, matrix products: 25.6 us -> 8.14 us  [the longest x1 2.79 us: shards(): jnp.dot(selector, tokens, preferred_element_type=jnp.float32)]
    all_gather x3 -> x0, local copies, waits for them, and re-layouts: 14.9 us -> none  [the longest x1 9.7 us: shards(): lax.all_gather(arrived, 'tp', axis=0, tiled=True).reshape(-1, features)]
    ppermute x0 -> x8, waiting for transfers between devices: none -> 7.7 us  [the longest x2 2.9 us: shards(): other = [lax.ppermute(rows, 'tp', swap) for rows in mine]]
  transfers between devices with their start and end apart: 11 -> 12, of which waited for: 9 -> 8; matrix products, arithmetic and copies ran while one was open for 5% -> 4% of each run, Pallas kernels for 10% -> 6%
where the time goes in v2:
time: 317 us; the launch traced here: 315 us
  waiting for transfers between devices  114 us (36%)
  blocking collectives  81.1 us (26%)
  Pallas kernels  57.3 us (18%)
  starting transfers between devices  18.4 us (6%)
  between operations  13.7 us (4%)
  other arithmetic  11.2 us (4%)
  local copies, waits for them, and re-layouts  10.8 us (3%)
  matrix products  8.14 us (3%)
    all_to_all x1, blocking collectives, shards(): lax.all_to_all(outgoing.reshape(experts, block, half), SP, split_axis=0,...  54.7 us
    all_gather x1, waiting for transfers between devices, shards(): gathered = lax.all_gather(packed, PLANE, axis=0)  40.7 us
    all_to_all x1, waiting for transfers between devices, shards(): lax.all_to_all(jnp.concatenate(summed, axis=0).reshape(experts, block, ha...  38.4 us
    pallas_call x1, Pallas kernels, flash(): pl.pallas_call(flash_body, grid=(blocks,), in_specs=[scalar, scalar, scal...  28.3 us
    all_to_all x1, waiting for transfers between devices, shards(): lax.all_to_all(parts, OWNERS, split_axis=0, concat_axis=0, tiled=True)  21.5 us
    pallas_call x2, Pallas kernels, expert(): pl.pallas_call(expert_body, grid=(count // block_rows,), in_specs=[pl.Blo...  19.4 us
    all_gather x1, blocking collectives, shards(): lax.all_gather(query_large.reshape(length, -1).T, 'z', axis=0)  13.3 us
    all_gather x1, blocking collectives, shards(): lax.all_gather(query_small.reshape(length, -1).T, 'z', axis=0)  13 us
  transfers between devices with their start and end apart: 12, of which 8 were waited for; matrix products, arithmetic and copies ran while one was open for 4% of the time, Pallas kernels for 6%

profile of v2, /device:TPU:4, one launch (start us, length us, event | category | flops | bytes accessed | tf_op | source)
XLA Modules:
  0.0 314.8 jit_solution(2864424342516777883)
XLA Ops:
  7.6 4.1 %collective-permute-start.2 = (bf16[384,384]{1,0:T(8,128)(2,1)S(1)}, bf16[384,384]{1,0:T(8,128)(2,1)S(1)}, u32[]{:S(2)}, u32[]{:S(2)}) collective-permute-start(bf16[384,384]{1,0:T(8,128)(2,1)S(1)} %pad_maximum_fusion.2), channel_id=1, source_target_pairs={{0,96},{32,64},{64,32},{96,0},{1,97},{33,65},{65,33},{97,1},{2,98}... | collective-permute-start | bytes 884744 | tf_op jit(solution)/shard_map/ppermute | solution.py:364
  12.7 6.0 %collective-permute-done.2 = bf16[384,384]{1,0:T(8,128)(2,1)S(1)} collective-permute-done((bf16[384,384]{1,0:T(8,128)(2,1)S(1)}, bf16[384,384]{1,0:T(8,128)(2,1)S(1)}, u32[]{:S(2)}, u32[]{:S(2)}) %collective-permute-start.2) | collective-permute-done | bytes 294944 | tf_op jit(solution)/shard_map/ppermute | solution.py:364
  18.9 1.8 pad_maximum_fusion.1
  20.7 13.3 %all-gather.1 = bf16[1024,384]{0,1:T(8,128)(2,1)S(1)} all-gather(bf16[256,384]{0,1:T(8,128)(2,1)S(1)} %bitcast.93), channel_id=3, replica_groups=mesh['z'=4,'y'=4,'x'=4,'tp'=2] {'z'}, dimensions={0}, use_global_device_ids=true | all-gather | bytes 983040 | tf_op jit(solution)/shard_map/all_gather | solution.py:375
  35.2 13.0 %all-gather = bf16[512,384]{0,1:T(8,128)(2,1)S(1)} all-gather(bf16[128,384]{0,1:T(8,128)(2,1)S(1)} %bitcast.95), channel_id=2, replica_groups=mesh['z'=4,'y'=4,'x'=4,'tp'=2] {'z'}, dimensions={0}, use_global_device_ids=true | all-gather | bytes 491520 | tf_op jit(solution)/shard_map/all_gather | solution.py:374
  49.7 40.7 %all-gather.5.cloned.1.call-done = bf16[10240,384]{1,0:T(8,128)(2,1)} async-done(((bf16[640,384]{1,0:T(8,128)(2,1)}), bf16[10240,384]{1,0:T(8,128)(2,1)}) %all-gather.5.cloned.1.call-update) | async-done | bytes 7864336 | tf_op jit(solution)/shard_map/all_gather | solution.py:373
  90.4 28.3 %shard_map.163 = bf16[4,384,640]{2,1,0:T(8,128)(2,1)} custom-call(s32[3]{0:T(128)} %pad_add_fusion.1.meta, f32[2]{0:T(128)} %bitcast.100, f32[2]{0:T(128)} %bitcast.101, bf16[4,128,384]{2,1,0:T(8,128)(2,1)} %bitcast.90, bf16[4,256,384]{2,1,0:T(8,128)(2,1)} %bitcast.89, bf16[16,640,384]{2,1,0:T(8,128)(2,1)} %bitcast.74, bf16[16,640,384]{2,1,0:T(8,128)(2,1)} %bitcast.75, ...), custom_call_target="tpu_custom_call" | custom-call | tf_op jit(solution)/shard_map/pallas_call | solution.py:150
  118.7 5.4 %all-to-all-start = ((bf16[8,192,640]{2,1,0:T(8,128)(2,1)}), bf16[8,192,640]{2,1,0:T(8,128)(2,1)S(1)}, u32[]{:S(2)}, u32[]{:S(2)}) async-start(bf16[8,192,640]{2,1,0:T(8,128)(2,1)} %bitcast.83), calls=%async_computation | async-start | bytes 3932160 | tf_op jit(solution)/shard_map/all_to_all | solution.py:407
  128.4 21.5 %all-to-all-done.arrived = bf16[8,192,640]{2,1,0:T(8,128)(2,1)S(1)} async-done(((bf16[8,192,640]{2,1,0:T(8,128)(2,1)}), bf16[8,192,640]{2,1,0:T(8,128)(2,1)S(1)}, u32[]{:S(2)}, u32[]{:S(2)}) %all-to-all-start) | async-done | bytes 1966112 | tf_op jit(solution)/shard_map/all_to_all | solution.py:407
  149.9 1.3 copy-done
  151.2 6.4 %shard_map.164 = (bf16[192,2048]{1,0:T(8,128)(2,1)}, bf16[192,1024]{1,0:T(8,128)(2,1)}, bf16[192,1024]{1,0:T(8,128)(2,1)}) custom-call(s32[1]{0:T(128)} %bitcast.core, bf16[8,192,640]{2,1,0:T(8,128)(2,1)} %copy-done, bf16[1,128]{1,0:T(2,128)(2,1)} %bitcast.99, bf16[192,2048]{1,0:T(8,128)(2,1)} %residual.1, bf16[512,2048]{1,0:T(8,128)(2,1)} %weight.1, ...), custom_call_target="tpu_custom_call" | custom-call | tf_op jit(solution)/shard_map/pallas_call | solution.py:238
  159.5 2.8 convolution_convert_fusion
  162.3 54.7 %all_to_all.15 = bf16[64,24,1024]{2,1,0:T(8,128)(2,1)S(1)} all-to-all(bf16[64,24,1024]{2,1,0:T(8,128)(2,1)S(1)} %bitcast.88), channel_id=1, replica_groups=mesh['z'=4,'y'=4,'x'=4,'tp'=2] {'z','y','x'}, dimensions={0} | all-to-all | bytes 6291456 | tf_op jit(solution)/shard_map/all_to_all | solution.py:415
  218.0 2.9 collective-permute-done.4.other
  222.0 9.7 %shard_map.165 = (bf16[768,1024]{1,0:T(8,128)(2,1)}, bf16[768,1024]{1,0:T(8,128)(2,1)}) custom-call(s32[1]{0:T(128)} %bitcast.core, bf16[768,1024]{1,0:T(8,128)(2,1)} %bitcast.87, bf16[768,1024]{1,0:T(8,128)(2,1)} %copy-done.6, bf16[1,2048,512]{2,1,0:T(8,128)(2,1)} %gate.3, bf16[1,2048,512]{2,1,0:T(8,128)(2,1)} %up.3, bf16[1,512,2048]{2,1,0:T(8,128)(2,1)} %down.3), custom_call_target="tpu_custom_call" | custom-call | tf_op jit(solution)/shard_map/pallas_call | solution.py:280
  233.2 9.7 %shard_map.166 = (bf16[768,1024]{1,0:T(8,128)(2,1)}, bf16[768,1024]{1,0:T(8,128)(2,1)}) custom-call(s32[1]{0:T(128)} %bitcast.core, bf16[768,1024]{1,0:T(8,128)(2,1)} %bitcast.85, bf16[768,1024]{1,0:T(8,128)(2,1)} %copy-done.5, bf16[1,2048,512]{2,1,0:T(8,128)(2,1)} %gate.3, bf16[1,2048,512]{2,1,0:T(8,128)(2,1)} %up.3, bf16[1,512,2048]{2,1,0:T(8,128)(2,1)} %down.3), custom_call_target="tpu_custom_call" | custom-call | tf_op jit(solution)/shard_map/pallas_call | solution.py:280
  244.0 2.6 collective-permute-done.7
  247.2 2.0 pad_maximum_fusion
  249.2 7.0 %all-to-all-start.2 = ((bf16[64,24,1024]{2,1,0:T(8,128)(2,1)}), bf16[64,24,1024]{2,1,0:T(8,128)(2,1)S(1)}, u32[]{:S(2)}, u32[]{:S(2)}) async-start(bf16[64,24,1024]{2,1,0:T(8,128)(2,1)} %bitcast.82), calls=%async_computation.2 | async-start | bytes 6291456 | tf_op jit(solution)/shard_map/all_to_all | solution.py:427
  257.6 2.2 fusion
  259.7 38.4 %all-to-all-done.2 = bf16[64,24,1024]{2,1,0:T(8,128)(2,1)S(1)} async-done(((bf16[64,24,1024]{2,1,0:T(8,128)(2,1)}), bf16[64,24,1024]{2,1,0:T(8,128)(2,1)S(1)}, u32[]{:S(2)}, u32[]{:S(2)}) %all-to-all-start.2) | async-done | bytes 3145760 | tf_op jit(solution)/shard_map/all_to_all | solution.py:427
  298.1 1.9 fusion.9
  302.2 1.7 convolution_add_fusion.1.own
  304.8 3.2 %shard_map.167 = bf16[192,2048]{1,0:T(8,128)(2,1)} custom-call(s32[1]{0:T(128)} %bitcast.core, f32[192,1024]{1,0:T(8,128)} %convolution_add_fusion.1.own, f32[192,1024]{1,0:T(8,128)} %copy-done.9, bf16[192,2048]{1,0:T(8,128)(2,1)} %get-tuple-element.18.middle, bf16[1,2048]{1,0:T(2,128)(2,1)} %get-tuple-element.25.norm_gain), custom_call_target="tpu_custom_call" | custom-call | tf_op jit(solution)/shard_map/pallas_call | solution.py:317
  (83 shorter events, 20.6 us)
Async XLA Ops:
  6.5 14.1 %copy-start.10 = (bf16[384,1,256]{2,0,1:T(8,128)(2,1)S(1)}, bf16[384,1,256]{2,0,1:T(8,128)(2,1)}, u32[]{:S(2)}) copy-start(bf16[384,1,256]{2,0,1:T(8,128)(2,1)} %param.20) | copy-start | bytes 589828
  6.5 83.9 %all-gather.5.cloned.1.call-start = ((), (), s32[]{:S(2)}) async-start(), calls=%async_computation.3 | async-start | bytes 8355840 | tf_op jit(solution)/shard_map/all_gather | solution.py:373
  7.6 11.1 %collective-permute-start.2 = (bf16[384,384]{1,0:T(8,128)(2,1)S(1)}, bf16[384,384]{1,0:T(8,128)(2,1)S(1)}, u32[]{:S(2)}, u32[]{:S(2)}) collective-permute-start(bf16[384,384]{1,0:T(8,128)(2,1)S(1)} %pad_maximum_fusion.2), channel_id=1, source_target_pairs={{0,96},{32,64},{64,32},{96,0},{1,97},{33,65},{65,33},{97,1},{2,98}... | collective-permute-start | bytes 884744 | tf_op jit(solution)/shard_map/ppermute | solution.py:364
  18.7 16.5 %copy-start.11 = (bf16[384,1,128]{2,0,1:T(8,128)(2,1)S(1)}, bf16[384,1,128]{2,0,1:T(8,128)(2,1)}, u32[]{:S(2)}) copy-start(bf16[384,1,128]{2,0,1:T(8,128)(2,1)} %param.17) | copy-start | bytes 294916
  118.7 5.4 %copy-start.13 = (s32[192,2]{0,1:T(2,128)S(1)}, s32[192,2]{0,1:T(2,128)}, u32[]{:S(2)}) copy-start(s32[192,2]{0,1:T(2,128)} %param.29) | copy-start | bytes 4612
  118.7 7.9 %copy-start.12 = (bf16[2,2048]{1,0:T(2,128)(2,1)S(1)}, bf16[2,2048]{1,0:T(2,128)(2,1)}, u32[]{:S(2)}) copy-start(bf16[2,2048]{1,0:T(2,128)(2,1)} %param.28) | copy-start | bytes 24580
  118.7 31.2 %all-to-all-start = ((bf16[8,192,640]{2,1,0:T(8,128)(2,1)}), bf16[8,192,640]{2,1,0:T(8,128)(2,1)S(1)}, u32[]{:S(2)}, u32[]{:S(2)}) async-start(bf16[8,192,640]{2,1,0:T(8,128)(2,1)} %bitcast.83), calls=%async_computation | async-start | bytes 3932160 | tf_op jit(solution)/shard_map/all_to_all | solution.py:407
  124.1 3.1 collective-permute-start
  149.9 1.3 copy-start
  157.6 1.9 collective-permute-start.3
  217.4 3.5 %copy-start.2 = (bf16[32,24,1024]{2,1,0:T(8,128)(2,1)}, bf16[32,24,1024]{2,1,0:T(8,128)(2,1)S(1)}, u32[]{:S(2)}) copy-start(bf16[32,24,1024]{2,1,0:T(8,128)(2,1)S(1)} %get-tuple-element.23) | copy-start | bytes 4718596
  217.4 14.4 %copy-start.1 = (bf16[32,24,1024]{2,1,0:T(8,128)(2,1)}, bf16[32,24,1024]{2,1,0:T(8,128)(2,1)S(1)}, u32[]{:S(2)}) copy-start(bf16[32,24,1024]{2,1,0:T(8,128)(2,1)S(1)} %get-tuple-element.24) | copy-start | bytes 4718596
  217.4 3.5 %collective-permute-start.4 = (bf16[768,1024]{1,0:T(8,128)(2,1)S(1)}, bf16[768,1024]{1,0:T(8,128)(2,1)S(1)}, u32[]{:S(2)}, u32[]{:S(2)}) collective-permute-start(bf16[768,1024]{1,0:T(8,128)(2,1)S(1)} %bitcast.86), channel_id=1, source_target_pairs={{0,1},{1,0},{2,3},{3,2},{4,5},{5,4},{6,7},{7,6},{8,9},{9,8},{10,11... | collective-permute-start | bytes 4718600 | tf_op jit(solution)/shard_map/ppermute | solution.py:421
  217.5 14.5 %collective-permute-start.6 = (bf16[768,1024]{1,0:T(8,128)(2,1)S(1)}, bf16[768,1024]{1,0:T(8,128)(2,1)S(1)}, u32[]{:S(2)}, u32[]{:S(2)}) collective-permute-start(bf16[768,1024]{1,0:T(8,128)(2,1)S(1)} %bitcast.84), channel_id=1, source_target_pairs={{0,1},{1,0},{2,3},{3,2},{4,5},{5,4},{6,7},{7,6},{8,9},{9,8},{10,11... | collective-permute-start | bytes 4718600 | tf_op jit(solution)/shard_map/ppermute | solution.py:421
  231.8 11.5 %copy-start.7 = (bf16[768,1024]{1,0:T(8,128)(2,1)S(1)}, bf16[768,1024]{1,0:T(8,128)(2,1)}, u32[]{:S(2)}) copy-start(bf16[768,1024]{1,0:T(8,128)(2,1)} %get-tuple-element.14) | copy-start | bytes 4718596
  231.8 11.5 %collective-permute-start.5 = (bf16[768,1024]{1,0:T(8,128)(2,1)}, bf16[768,1024]{1,0:T(8,128)(2,1)S(1)}, u32[]{:S(2)}, u32[]{:S(2)}) collective-permute-start(bf16[768,1024]{1,0:T(8,128)(2,1)} %get-tuple-element.15), channel_id=1, source_target_pairs={{0,1},{1,0},{2,3},{3,2},{4,5},{5,4},{6,7},{7,6},{8,9},{9,8},{10,11... | collective-permute-start | bytes 4718600 | tf_op jit(solution)/shard_map/ppermute | solution.py:425
  242.9 3.6 %collective-permute-start.7 = (bf16[768,1024]{1,0:T(8,128)(2,1)}, bf16[768,1024]{1,0:T(8,128)(2,1)S(1)}, u32[]{:S(2)}, u32[]{:S(2)}) collective-permute-start(bf16[768,1024]{1,0:T(8,128)(2,1)} %get-tuple-element.17), channel_id=1, source_target_pairs={{0,1},{1,0},{2,3},{3,2},{4,5},{5,4},{6,7},{7,6},{8,9},{9,8},{10,11... | collective-permute-start | bytes 4718600 | tf_op jit(solution)/shard_map/ppermute | solution.py:425
  243.3 3.2 %copy-start.8 = (bf16[768,1024]{1,0:T(8,128)(2,1)S(1)}, bf16[768,1024]{1,0:T(8,128)(2,1)}, u32[]{:S(2)}) copy-start(bf16[768,1024]{1,0:T(8,128)(2,1)} %get-tuple-element.16) | copy-start | bytes 4718596
  249.2 7.1 %copy-start.14 = (f32[192,2]{0,1:T(2,128)S(1)}, f32[192,2]{0,1:T(2,128)}, u32[]{:S(2)}) copy-start(f32[192,2]{0,1:T(2,128)} %param.30) | copy-start | bytes 4612
  249.2 49.0 %all-to-all-start.2 = ((bf16[64,24,1024]{2,1,0:T(8,128)(2,1)}), bf16[64,24,1024]{2,1,0:T(8,128)(2,1)S(1)}, u32[]{:S(2)}, u32[]{:S(2)}) async-start(bf16[64,24,1024]{2,1,0:T(8,128)(2,1)} %bitcast.82), calls=%async_computation.2 | async-start | bytes 6291456 | tf_op jit(solution)/shard_map/all_to_all | solution.py:427
  256.2 1.2 collective-permute-start.1
  298.1 1.9 copy-start.4
  300.1 1.3 copy-start.3
  300.9 3.0 collective-permute-start.8
  (3 other events, 3.3 us)
Sparse Core Ops, SparseCore 0:
  20.8 69.5 all-gather.4
